TPU v7x, 512 devices: a whole 4x4x16 slice. The times are simulated.
512 devices in a mesh: ep: 32 (over z, core), tp: 16 (over y, x).
Axes of the slice: x: 4, y: 4, z: 16, core: 2. Of those that a mesh axis runs over, the one named last changes fastest.
Arguments:
- query_rows: bfloat16 [24576, 1024], P('ep', 'tp'), may hold values from -600 to 600
- key_rows: bfloat16 [24576, 1024], P('ep', 'tp'), may hold values from -6 to 6
- value_rows: bfloat16 [24576, 1024], P('ep', 'tp'), may hold values from -6 to 6
- cum_gate: float32 [16, 24576], P('tp'), may hold values from -2458 to 0, as said below
- out_weight: bfloat16 [1024, 2048], P(None, 'tp'), may hold values from -0.1875 to 0.1875
- moe_input: bfloat16 [6144, 2048], P('ep'), may hold values from -6 to 6
- moe_gain: float32 [2048], replicated, may hold values from 0.1 to 1.9
- routes: int32 [6144, 3], P('ep'), may hold values from 0 to 127, all different within a row; in each aligned block of 192 rows (0 to 191, 192 to 383, ...) at most 9 rows name the same one
- route_weight: float32 [6144, 3], P('ep'), may hold values from 0.2 to 1.5
- expert_gate: bfloat16 [128, 2048, 512], P('ep', None, 'tp'), may hold values from -0.125 to 0.125
- expert_up: bfloat16 [128, 2048, 512], P('ep', None, 'tp'), may hold values from -0.125 to 0.125
- expert_down: bfloat16 [128, 512, 2048], P('ep', None, 'tp'), may hold values from -0.25 to 0.25
- shared_gate: bfloat16 [2048, 512], P(None, 'tp'), may hold values from -0.125 to 0.125
- shared_up: bfloat16 [2048, 512], P(None, 'tp'), may hold values from -0.125 to 0.125
- shared_down: bfloat16 [512, 2048], P(None, 'tp'), may hold values from -0.25 to 0.25
Outputs:
- mixer_out: bfloat16 [24576, 2048], P('ep', 'tp')
- moe_out: bfloat16 [6144, 2048], P('ep', 'tp')
Inputs may be any that keep to these rules, and one draw needn't show every extreme that they name: Non-increasing along positions: cum_gate[h, t] is the sum of the log forget gates of head h over positions 0 to t. `routes`: the 3 experts of a token differ. In each aligned block of 192 tokens no expert is named by more than 9 tokens, a bound that some block reaches.
All inputs are finite; a program needn't handle non-finite values.
Results may differ from a plain program's by a relative error of at most 0.0068.
Values may be sent and summed in bfloat16 or wider, within the bound.
No kernel may reach another device: no remote copies, remote signals or barrier semaphores. Data moves between devices by JAX's collectives and lax.ppermute only.
A program may use at most 64 MiB of HBM per device.

v0:
```python
import jax
import jax.numpy as jnp
from jax import lax
from jax.sharding import PartitionSpec as P

HEAD = 64
neg_fill = -1e30
norm_eps = 1e-06


def joined_along(pieces, dim):
    dims = list(pieces.shape[1:])
    dims[dim] *= pieces.shape[0]
    return jnp.moveaxis(pieces, 0, dim).reshape(dims)


def sent_to_all(array, axis):
    copies = jnp.broadcast_to(array, (lax.axis_size(axis), *array.shape))
    return lax.all_to_all(copies, axis, split_axis=0, concat_axis=0, tiled=True)


def collect(array, axis, dim):
    return joined_along(sent_to_all(array, axis), dim)


def local(
    query_rows,
    key_rows,
    value_rows,
    cum_gate,
    out_weight,
    moe_input,
    moe_gain,
    routes,
    route_weight,
    expert_gate,
    expert_up,
    expert_down,
    shared_gate,
    shared_up,
    shared_down,
):
    row_count = query_rows.shape[0]
    width = query_rows.shape[1]
    local_heads = width // HEAD
    scale = HEAD ** (-0.5)
    first_row = lax.axis_index("ep") * row_count
    last_row = first_row + row_count - 1
    query_heads = query_rows.reshape(row_count, local_heads, HEAD)
    query_gate = lax.dynamic_slice_in_dim(cum_gate, first_row, row_count, 1)
    query_pos = first_row + jnp.arange(row_count, dtype=jnp.int32)
    key_value = jnp.concatenate([key_rows, value_rows], axis=1)
    initial = (
        jnp.full((local_heads, row_count), neg_fill, jnp.float32),
        jnp.zeros((local_heads, row_count), jnp.float32),
        jnp.zeros((local_heads, row_count, HEAD), jnp.float32),
    )
    shard_rows = lax.all_gather(key_value, "ep", axis=0, tiled=True)
    piece_len = shard_rows.shape[0]
    key_span = 512

    def one_span(state_in, span_index):
        span_start = span_index * key_span

        def update(state_old):
            running_max, denominator, weighted = state_old
            block = lax.dynamic_slice_in_dim(shard_rows, span_index * key_span, key_span, 0)
            keys_block = block[:, :width].reshape(key_span, local_heads, HEAD)
            values_block = block[:, width:].reshape(key_span, local_heads, HEAD)
            key_gate = lax.dynamic_slice_in_dim(cum_gate, span_start, key_span, 1)
            scores = (
                jnp.einsum(
                    "qhd,khd->hqk", query_heads, keys_block, preferred_element_type=jnp.float32
                )
                * scale
            )
            scores = scores + query_gate[:, :, None] - key_gate[:, None, :]
            causal = (span_start + jnp.arange(key_span, dtype=jnp.int32))[None, :] <= query_pos[
                :, None
            ]
            scores = jnp.where(causal[None], scores, neg_fill)
            new_max = jnp.maximum(running_max, jnp.max(scores, axis=2))
            expon = jnp.where(causal[None], jnp.exp(scores - new_max[:, :, None]), 0.0)
            rescale = jnp.exp(running_max - new_max)
            denominator = denominator * rescale + jnp.sum(expon, axis=2)
            weighted = weighted * rescale[:, :, None] + jnp.einsum(
                "hqk,khd->hqd",
                expon.astype(jnp.bfloat16),
                values_block,
                preferred_element_type=jnp.float32,
            )
            return (new_max, denominator, weighted)

        state_next = lax.cond(span_start <= last_row, update, lambda unchanged: unchanged, state_in)
        return (state_next, None)

    state_out, _ = lax.scan(one_span, initial, jnp.arange(piece_len // key_span, dtype=jnp.int32))
    running_max, denominator, weighted = state_out
    heads_out = (weighted / denominator[:, :, None]).transpose(1, 0, 2).reshape(row_count, width)
    heads_out = heads_out.astype(jnp.bfloat16)
    token_count = moe_input.shape[0]
    top_count = routes.shape[1]
    local_experts = expert_gate.shape[0]
    ep_count = lax.axis_size("ep")
    expert_count = local_experts * ep_count
    capacity = 2 * token_count * top_count // expert_count
    column_count = expert_down.shape[2]
    first_column = lax.axis_index("tp") * column_count
    moe_rows = moe_input.astype(jnp.float32)
    normed = (
        moe_rows
        * lax.rsqrt(jnp.mean(moe_rows * moe_rows, axis=1, keepdims=True) + norm_eps)
        * moe_gain
    ).astype(jnp.bfloat16)
    flat_routes = routes.reshape(-1)
    one_hot = (flat_routes[:, None] == jnp.arange(expert_count, dtype=jnp.int32)[None, :]).astype(
        jnp.int32
    )
    ranks = jnp.sum(jnp.cumsum(one_hot, axis=0) * one_hot, axis=1) - 1
    slot_index = flat_routes * capacity + ranks
    pair_token = jnp.arange(token_count * top_count, dtype=jnp.int32) // top_count
    slot_token = (
        jnp.full((expert_count * capacity,), token_count, jnp.int32).at[slot_index].set(pair_token)
    )
    padded = jnp.concatenate([normed, jnp.zeros((1, normed.shape[1]), jnp.bfloat16)], axis=0)
    outgoing = lax.dynamic_slice_in_dim(padded, first_column, column_count, 1)[slot_token]
    outgoing = outgoing.reshape(ep_count, local_experts, capacity, outgoing.shape[1])
    arrived = lax.all_to_all(outgoing, "ep", split_axis=0, concat_axis=0, tiled=True)
    arrived = lax.all_gather(arrived, "tp", axis=3, tiled=True)
    gate_val = jnp.einsum(
        "aecd,edf->aecf", arrived, expert_gate, preferred_element_type=jnp.float32
    )
    up_val = jnp.einsum("aecd,edf->aecf", arrived, expert_up, preferred_element_type=jnp.float32)
    hidden = (jax.nn.silu(gate_val) * up_val).astype(jnp.bfloat16)
    hidden = collect(hidden, "tp", 3)
    result = jnp.einsum(
        "aecf,efd->aecd", hidden, expert_down, preferred_element_type=jnp.float32
    ).astype(jnp.bfloat16)
    returned = lax.all_to_all(result, "ep", split_axis=0, concat_axis=0, tiled=True)
    picked = returned.reshape(expert_count * capacity, column_count)[slot_index]
    picked = picked.astype(jnp.float32).reshape(token_count, top_count, column_count)
    routed = jnp.sum(picked * route_weight[:, :, None], axis=1)
    shared_hidden = (
        jax.nn.silu(jnp.dot(normed, shared_gate, preferred_element_type=jnp.float32))
        * jnp.dot(normed, shared_up, preferred_element_type=jnp.float32)
    ).astype(jnp.bfloat16)
    mixer_sum = jnp.dot(
        lax.all_gather(heads_out, "tp", axis=1, tiled=True),
        out_weight,
        preferred_element_type=jnp.float32,
    )
    shared_all = lax.all_gather(shared_hidden, "tp", axis=1, tiled=True)
    moe_total = routed + jnp.dot(shared_all, shared_down, preferred_element_type=jnp.float32)
    return (mixer_sum.astype(jnp.bfloat16), moe_total.astype(jnp.bfloat16))


def solution(mesh):
    placed = (
        P("ep", "tp"),
        P("ep", "tp"),
        P("ep", "tp"),
        P("tp", None),
        P(None, "tp"),
        P("ep", None),
        P(),
        P("ep", None),
        P("ep", None),
        P("ep", None, "tp"),
        P("ep", None, "tp"),
        P("ep", None, "tp"),
        P(None, "tp"),
        P(None, "tp"),
        P(None, "tp"),
    )
    return jax.shard_map(
        local, mesh=mesh, in_specs=placed, out_specs=(P("ep", "tp"), P("ep", "tp")), check_vma=False
    )
```

profile of v0, /device:TPU:1, one launch (start us, length us, event | category | flops | bytes accessed | tf_op | source)
XLA Modules:
  0.0 554.8 jit_solution(1330439696241112962)
XLA Ops:
  11.6 4.1 scatter_custom_fusion
  16.0 2.9 gather_fusion
  19.3 40.2 %all_to_all.15 = bf16[32,4,9,128]{3,1,2,0:T(4,128)(2,1)S(1)} all-to-all(bf16[32,4,9,128]{3,1,2,0:T(4,128)(2,1)S(1)} %copy.46), channel_id=1, replica_groups=mesh['ep'=32,'tp'=16] {'ep'}, dimensions={0} | all-to-all | bytes 589824 | tf_op jit(solution)/shard_map/all_to_all | solution.py:128
  61.6 63.6 %all-gather.7.cloned.1.call-done = bf16[32,4,9,2048]{3,0,2,1:T(8,128)(2,1)} async-done(((bf16[32,4,9,128]{3,0,2,1:T(8,128)(2,1)}), bf16[32,4,9,2048]{3,0,2,1:T(8,128)(2,1)}) %all-gather.7.cloned.1.call-update) | async-done | bytes 4718608 | tf_op jit(solution)/shard_map/all_gather | solution.py:129
  125.2 3.8 convolution_bitcast_fusion.2
  130.5 3.2 broadcast_bitcast_fusion
  133.7 7.8 %reshape.164 = bf16[16,2,18432]{2,1,0:T(2,128)(2,1)} reshape(bf16[16,4,9,32,32]{4,3,2,1,0:T(8,128)(2,1)} %broadcast_bitcast_fusion) | data formatting | bytes 2359296
  141.5 4.8 all-to-all-start.1
  147.2 58.1 %all-gather.5.cloned.1.call-done = bf16[24576,128]{1,0:T(8,128)(2,1)} async-done(((bf16[768,128]{1,0:T(8,128)(2,1)}), bf16[24576,128]{1,0:T(8,128)(2,1)}) %all-gather.5.cloned.1.call-update) | async-done | bytes 6291472 | tf_op jit(solution)/shard_map/all_gather | solution.py:58
  205.4 76.2 %while.15 = (s32[]{:T(128)}, f32[1,768]{1,0:T(1,128)S(1)}, f32[1,768]{1,0:T(1,128)S(1)}, f32[1,768,64]{1,2,0:T(8,128)S(1)}, s32[48]{0:T(128)S(1)}, /*index=5*/s3...) while((s32[]{:T(128)}, f32[1,768]{1,0:T(1,128)S(1)}, ...), condition=%wide.region_5.6_spmd.clone, body=%wide.region_0.5_spmd.clone.sunk | while | flops 106270224 | bytes 5566899 | solution.py:97
  206.7 4.7 conditional.3
  209.6 1.4 fusion.4
  212.6 4.7 conditional.3
  215.5 1.4 fusion.4
  218.6 4.7 conditional.3
  282.3 3.8 reshape.165
  286.1 3.1 bitcast_bitcast_fusion
  289.2 7.6 %copy.48 = bf16[32,4,9,16,32]{4,3,0,2,1:T(8,128)(2,1)} copy(bf16[32,4,9,16,32]{4,0,2,1,3:T(8,128)(2,1)S(1)} %bitcast_bitcast_fusion) | data formatting | bytes 2359296 | tf_op jit(solution)/shard_map/transpose | solution.py:14
  296.8 6.5 %reshape.124 = bf16[32,4,9,512]{3,0,2,1:T(8,128)(2,1)S(1)} reshape(bf16[32,4,9,16,32]{4,3,0,2,1:T(8,128)(2,1)} %copy.48) | data formatting | bytes 2359296 | tf_op jit(solution)/shard_map/reshape | solution.py:14
  304.7 213.7 %all-to-all-start.2 = ((bf16[32,4,9,128]{3,1,2,0:T(4,128)(2,1)}), bf16[32,4,9,128]{3,1,2,0:T(4,128)(2,1)S(1)}, u32[]{:S(2)}, u32[]{:S(2)}) async-start(bf16[32,4,9,128]{3,1,2,0:T(4,128)(2,1)} %copy.49), calls=%async_computation.2 | async-start | bytes 589824 | tf_op jit(solution)/shard_map/all_to_all | solution.py:139
  519.2 20.5 %all_gather.15 = bf16[192,512]{0,1:T(8,128)(2,1)S(1)} all-gather(bf16[192,32]{0,1:T(8,128)(2,1)S(1)} %fusion.27), channel_id=1, replica_groups=mesh['ep'=32,'tp'=16] {'tp'}, dimensions={1}, use_global_device_ids=true | all-gather | bytes 208896 | tf_op jit(solution)/shard_map/all_gather | solution.py:152
  539.7 2.2 all-to-all-done.2
  542.2 1.9 gather_fusion.1
  545.5 2.7 fusion.22
  (252 shorter events, 51.7 us)
Async XLA Ops:
  7.2 296.1 %copy-start = (bf16[4,512,128]{2,1,0:T(8,128)(2,1)S(1)}, bf16[4,512,128]{2,1,0:T(8,128)(2,1)}, u32[]{:S(2)}) copy-start(bf16[4,512,128]{2,1,0:T(8,128)(2,1)} %param.30) | copy-start | bytes 1572868
  7.2 118.0 %all-gather.7.cloned.1.call-start = ((), (), s32[]{:S(2)}) async-start(), calls=%async_computation.4 | async-start | bytes 5013504 | tf_op jit(solution)/shard_map/all_gather | solution.py:129
  10.9 4.8 copy-start.1
  10.9 4.8 copy-start.8
  19.0 41.4 %copy-start.6 = (bf16[768,64]{0,1:T(8,128)(2,1)S(1)}, bf16[768,64]{0,1:T(8,128)(2,1)}, u32[]{:S(2)}) copy-start(bf16[768,64]{0,1:T(8,128)(2,1)} %param.20) | copy-start | bytes 294916
  19.0 41.6 %copy-start.7 = (bf16[768,64]{0,1:T(8,128)(2,1)S(1)}, bf16[768,64]{0,1:T(8,128)(2,1)}, u32[]{:S(2)}) copy-start(bf16[768,64]{0,1:T(8,128)(2,1)} %param.21) | copy-start | bytes 294916
  19.3 105.9 %copy-start.11 = (bf16[4,2048,32]{1,2,0:T(8,128)(2,1)S(1)}, bf16[4,2048,32]{1,2,0:T(8,128)(2,1)}, u32[]{:S(2)}) copy-start(bf16[4,2048,32]{1,2,0:T(8,128)(2,1)} %param.28) | copy-start | bytes 1572868
  60.3 145.0 %all-gather.5.cloned.1.call-start = ((), (), s32[]{:S(2)}) async-start(), calls=%async_computation.3 | async-start | bytes 6488064 | tf_op jit(solution)/shard_map/all_gather | solution.py:58
  61.6 67.5 %copy-start.12 = (bf16[4,2048,32]{1,2,0:T(8,128)(2,1)S(1)}, bf16[4,2048,32]{1,2,0:T(8,128)(2,1)}, u32[]{:S(2)}) copy-start(bf16[4,2048,32]{1,2,0:T(8,128)(2,1)} %param.29) | copy-start | bytes 1572868
  125.2 3.9 copy-start.10
  141.5 63.9 %copy-start.13 = (bf16[768,64]{0,1:T(8,128)(2,1)S(1)}, bf16[768,64]{0,1:T(8,128)(2,1)}, u32[]{:S(2)}) copy-start(bf16[768,64]{0,1:T(8,128)(2,1)} %param.19) | copy-start | bytes 294916
  141.5 140.8 %all-to-all-start.1 = ((bf16[16,2,18432]{2,1,0:T(2,128)(2,1)}), bf16[16,2,18432]{2,1,0:T(2,128)(2,1)S(1)}, u32[]{:S(2)}, u32[]{:S(2)}) async-start(bf16[16,2,18432]{2,1,0:T(2,128)(2,1)} %reshape.164), calls=%async_computation.1 | async-start | bytes 2359296 | tf_op jit(solution)/shard_map/all_to_all | solution.py:19
  146.3 399.2 %all-gather.9.cloned.1.call-start = ((), (), s32[]{:S(2)}) async-start(), calls=%async_computation.5 | async-start | bytes 1671168 | tf_op jit(solution)/shard_map/all_gather | solution.py:148
  303.3 215.1 %copy-start.9 = (f32[192,3]{0,1:T(4,128)S(1)}, f32[192,3]{0,1:T(4,128)}, u32[]{:S(2)}) copy-start(f32[192,3]{0,1:T(4,128)} %param.27) | copy-start | bytes 6916
  303.3 215.2 %copy-start.4 = (bf16[2048,32]{0,1:T(8,128)(2,1)S(1)}, bf16[2048,32]{0,1:T(8,128)(2,1)}, u32[]{:S(2)}) copy-start(bf16[2048,32]{0,1:T(8,128)(2,1)} %param.31) | copy-start | bytes 393220
  303.8 215.1 %copy-start.5 = (bf16[2048,32]{0,1:T(8,128)(2,1)S(1)}, bf16[2048,32]{0,1:T(8,128)(2,1)}, u32[]{:S(2)}) copy-start(bf16[2048,32]{0,1:T(8,128)(2,1)} %param.32) | copy-start | bytes 393220
  304.7 237.3 %all-to-all-start.2 = ((bf16[32,4,9,128]{3,1,2,0:T(4,128)(2,1)}), bf16[32,4,9,128]{3,1,2,0:T(4,128)(2,1)S(1)}, u32[]{:S(2)}, u32[]{:S(2)}) async-start(bf16[32,4,9,128]{3,1,2,0:T(4,128)(2,1)} %copy.49), calls=%async_computation.2 | async-start | bytes 589824 | tf_op jit(solution)/shard_map/all_to_all | solution.py:139
  542.1 2.6 copy-start.3
  542.2 3.3 copy-start.2
Sparse Core Ops, SparseCore 0:
  60.4 64.7 all-gather.6
  127.9 77.4 all-gather.4
  282.4 260.1 all-gather.8
where the time goes:
time: 559 us; the launch traced here: 555 us
  starting transfers between devices  219 us (39%)
  waiting for transfers between devices  124 us (22%)
  local copies, waits for them, and re-layouts  76.5 us (14%)
  blocking collectives  60.7 us (11%)
  loops' own time  36.1 us (6%)
  matrix products  18.3 us (3%)
  between operations  14.2 us (3%)
  other arithmetic  6.13 us (1%)
    all_to_all x1, starting transfers between devices, local(): lax.all_to_all(result, 'ep', split_axis=0, concat_axis=0, tiled=True)  214 us
    all_gather x1, waiting for transfers between devices, local(): arrived = lax.all_gather(arrived, 'tp', axis=3, tiled=True)  63.6 us
    all_gather x1, waiting for transfers between devices, local(): shard_rows = lax.all_gather(key_value, 'ep', axis=0, tiled=True)  58.1 us
    all_to_all x1, blocking collectives, local(): lax.all_to_all(outgoing, 'ep', split_axis=0, concat_axis=0, tiled=True)  40.2 us
    another operation x1, loops' own time, local(): lax.scan(one_span, initial, jnp.arange(piece_len // key_span, dtype=jnp.i...  33.2 us
    dynamic_slice x48, local copies, waits for them, and re-layouts, local(): lax.scan(one_span, initial, jnp.arange(piece_len // key_span, dtype=jnp.i...  28.1 us
    all_gather x1, blocking collectives, local(): shared_all = lax.all_gather(shared_hidden, 'tp', axis=1, tiled=True)  20.5 us
    unnamed x35, local copies, waits for them, and re-layouts  16.1 us
  transfers between devices with their start and end apart: 5, of which 3 were waited for; matrix products, arithmetic and copies ran while one was open for 15% of the time, Pallas kernels for 0%

commit v1 on v0

--- a/solution.py
+++ b/solution.py
@@ -6,6 +6,26 @@
 HEAD = 64
 neg_fill = -1e30
 norm_eps = 1e-06
+
+
+def _serve_skins(q_in):
+    ax_name = "tp"
+    r2 = lax.axis_index(ax_name)
+    value_now = lax.axis_size(ax_name)
+    w2, part_now, res = (value_now, r2, q_in.shape[3])
+    blocks_here = [(rr, (rr + 1) % w2) for rr in range(w2)]
+    column = [(rr, (rr - 1) % w2) for rr in range(w2)]
+    b_now = jnp.zeros((*q_in.shape[:3], w2 * res, *q_in.shape[4:]), q_in.dtype)
+    b_now = lax.dynamic_update_slice_in_dim(b_now, q_in, part_now * res, axis=3)
+    lower = z1 = q_in
+    current_block = w2 // 2
+    for b in range(1, current_block + 1):
+        lower = lax.ppermute(lower, ax_name, blocks_here)
+        b_now = lax.dynamic_update_slice_in_dim(b_now, lower, (part_now - b) % w2 * res, axis=3)
+        if b < w2 - current_block:
+            z1 = lax.ppermute(z1, ax_name, column)
+            b_now = lax.dynamic_update_slice_in_dim(b_now, z1, (part_now + b) % w2 * res, axis=3)
+    return b_now
 
 
 def joined_along(pieces, dim):
@@ -126,7 +146,7 @@
     outgoing = lax.dynamic_slice_in_dim(padded, first_column, column_count, 1)[slot_token]
     outgoing = outgoing.reshape(ep_count, local_experts, capacity, outgoing.shape[1])
     arrived = lax.all_to_all(outgoing, "ep", split_axis=0, concat_axis=0, tiled=True)
-    arrived = lax.all_gather(arrived, "tp", axis=3, tiled=True)
+    arrived = _serve_skins(arrived)
     gate_val = jnp.einsum(
         "aecd,edf->aecf", arrived, expert_gate, preferred_element_type=jnp.float32
     )

time: 559 us -> 531 us (0.950)
  waiting for transfers between devices: 124 us -> 26.1 us
  starting transfers between devices: 219 us -> 282 us
  local copies, waits for them, and re-layouts: 76.5 us -> 83.2 us
    all_gather x1 -> x0, waiting for transfers between devices: 63.6 us -> none  [local(): arrived = lax.all_gather(arrived, 'tp', axis=3, tiled=True)]
    ppermute x0 -> x15, starting transfers between devices: none -> 62.4 us  [the longest x7 45.8 us: _serve_skins(): z1 = lax.ppermute(z1, ax_name, column)]
    all_gather x1, waiting for transfers between devices: 58.1 us -> 0.01 us  [local(): shard_rows = lax.all_gather(key_value, 'ep', axis=0, tiled=True)]
    ppermute x0 -> x15, waiting for transfers between devices: none -> 24.2 us  [the longest x8 24.2 us: _serve_skins(): lower = lax.ppermute(lower, ax_name, blocks_here)]
    unnamed x35 -> x31, local copies, waits for them, and re-layouts: 16.1 us -> 21.1 us
  transfers between devices with their start and end apart: 5 -> 19, of which waited for: 3 -> 9; matrix products, arithmetic and copies ran while one was open for 15% -> 19% of each run, Pallas kernels for 0% -> 0%
where the time goes in v1:
time: 531 us; the launch traced here: 526 us
  starting transfers between devices  282 us (53%)
  local copies, waits for them, and re-layouts  83.2 us (16%)
  blocking collectives  63.1 us (12%)
  loops' own time  35.9 us (7%)
  waiting for transfers between devices  26.1 us (5%)
  matrix products  15.8 us (3%)
  between operations  15.1 us (3%)
    all_to_all x1, starting transfers between devices, local(): lax.all_to_all(result, 'ep', split_axis=0, concat_axis=0, tiled=True)  215 us
    ppermute x7, starting transfers between devices, _serve_skins(): z1 = lax.ppermute(z1, ax_name, column)  45.8 us
    all_to_all x1, blocking collectives, local(): lax.all_to_all(outgoing, 'ep', split_axis=0, concat_axis=0, tiled=True)  42.2 us
    another operation x1, loops' own time, local(): lax.scan(one_span, initial, jnp.arange(piece_len // key_span, dtype=jnp.i...  33.1 us
    dynamic_slice x48, local copies, waits for them, and re-layouts, local(): lax.scan(one_span, initial, jnp.arange(piece_len // key_span, dtype=jnp.i...  28.2 us
    ppermute x8, waiting for transfers between devices, _serve_skins(): lower = lax.ppermute(lower, ax_name, blocks_here)  24.2 us
    unnamed x31, local copies, waits for them, and re-layouts  21.1 us
    all_gather x1, blocking collectives, local(): shared_all = lax.all_gather(shared_hidden, 'tp', axis=1, tiled=True)  20.9 us
  transfers between devices with their start and end apart: 19, of which 9 were waited for; matrix products, arithmetic and copies ran while one was open for 19% of the time, Pallas kernels for 0%

profile of v1, /device:TPU:1, one launch (start us, length us, event | category | flops | bytes accessed | tf_op | source)
XLA Modules:
  0.0 525.8 jit_solution(16659211299161667795)
XLA Ops:
  12.5 4.1 scatter_custom_fusion
  20.4 42.2 %all_to_all.15 = bf16[32,4,9,128]{3,1,2,0:T(4,128)(2,1)S(1)} all-to-all(bf16[32,4,9,128]{3,1,2,0:T(4,128)(2,1)S(1)} %copy.78), channel_id=1, replica_groups=mesh['ep'=32,'tp'=16] {'ep'}, dimensions={0} | all-to-all | bytes 589824 | tf_op jit(solution)/shard_map/all_to_all | solution.py:148
  65.7 5.7 %collective-permute-start.1 = (bf16[32,4,9,128]{3,1,2,0:T(4,128)(2,1)S(1)}, bf16[32,4,9,128]{3,1,2,0:T(4,128)(2,1)S(1)}, u32[]{:S(2)}, u32[]{:S(2)}) collective-permute-start(bf16[32,4,9,128]{3,1,2,0:T(4,128)(2,1)S(1)} %all_to_all.15), channel_id=1, source_target_pairs={{0,15},{1,0},{2,1},{3,2},{4,3},{5,4},{6,5},{7,6},{8,7},{9,8},{10,9... | collective-permute-start | bytes 884744 | tf_op jit(solution)/shard_map/ppermute | solution.py:26
  72.4 3.1 collective-permute-done
  77.4 6.7 %collective-permute-start.3 = (bf16[32,4,9,128]{3,1,2,0:T(4,128)(2,1)S(1)}, bf16[32,4,9,128]{3,1,2,0:T(4,128)(2,1)S(1)}, u32[]{:S(2)}, u32[]{:S(2)}) collective-permute-start(bf16[32,4,9,128]{3,1,2,0:T(4,128)(2,1)S(1)} %collective-permute-done.1), channel_id=1, source_target_pairs={{0,15},{1,0},{2,1},{3,2},{4,3},{5,4},{6,5},{7,6},{8,7},{9,8},{10,9... | collective-permute-start | bytes 884744 | tf_op jit(solution)/shard_map/ppermute | solution.py:26
  89.2 6.7 %collective-permute-start.5 = (bf16[32,4,9,128]{3,1,2,0:T(4,128)(2,1)S(1)}, bf16[32,4,9,128]{3,1,2,0:T(4,128)(2,1)S(1)}, u32[]{:S(2)}, u32[]{:S(2)}) collective-permute-start(bf16[32,4,9,128]{3,1,2,0:T(4,128)(2,1)S(1)} %collective-permute-done.3), channel_id=1, source_target_pairs={{0,15},{1,0},{2,1},{3,2},{4,3},{5,4},{6,5},{7,6},{8,7},{9,8},{10,9... | collective-permute-start | bytes 884744 | tf_op jit(solution)/shard_map/ppermute | solution.py:26
  100.0 6.7 %collective-permute-start.7 = (bf16[32,4,9,128]{3,1,2,0:T(4,128)(2,1)S(1)}, bf16[32,4,9,128]{3,1,2,0:T(4,128)(2,1)S(1)}, u32[]{:S(2)}, u32[]{:S(2)}) collective-permute-start(bf16[32,4,9,128]{3,1,2,0:T(4,128)(2,1)S(1)} %collective-permute-done.5), channel_id=1, source_target_pairs={{0,15},{1,0},{2,1},{3,2},{4,3},{5,4},{6,5},{7,6},{8,7},{9,8},{10,9... | collective-permute-start | bytes 884744 | tf_op jit(solution)/shard_map/ppermute | solution.py:26
  110.8 6.7 %collective-permute-start.9 = (bf16[32,4,9,128]{3,1,2,0:T(4,128)(2,1)S(1)}, bf16[32,4,9,128]{3,1,2,0:T(4,128)(2,1)S(1)}, u32[]{:S(2)}, u32[]{:S(2)}) collective-permute-start(bf16[32,4,9,128]{3,1,2,0:T(4,128)(2,1)S(1)} %collective-permute-done.7), channel_id=1, source_target_pairs={{0,15},{1,0},{2,1},{3,2},{4,3},{5,4},{6,5},{7,6},{8,7},{9,8},{10,9... | collective-permute-start | bytes 884744 | tf_op jit(solution)/shard_map/ppermute | solution.py:26
  121.6 6.7 %collective-permute-start.11 = (bf16[32,4,9,128]{3,1,2,0:T(4,128)(2,1)S(1)}, bf16[32,4,9,128]{3,1,2,0:T(4,128)(2,1)S(1)}, u32[]{:S(2)}, u32[]{:S(2)}) collective-permute-start(bf16[32,4,9,128]{3,1,2,0:T(4,128)(2,1)S(1)} %collective-permute-done.9), channel_id=1, source_target_pairs={{0,15},{1,0},{2,1},{3,2},{4,3},{5,4},{6,5},{7,6},{8,7},{9,8},{10,9... | collective-permute-start | bytes 884744 | tf_op jit(solution)/shard_map/ppermute | solution.py:26
  132.3 6.7 %collective-permute-start.13 = (bf16[32,4,9,128]{3,1,2,0:T(4,128)(2,1)S(1)}, bf16[32,4,9,128]{3,1,2,0:T(4,128)(2,1)S(1)}, u32[]{:S(2)}, u32[]{:S(2)}) collective-permute-start(bf16[32,4,9,128]{3,1,2,0:T(4,128)(2,1)S(1)} %collective-permute-done.11), channel_id=1, source_target_pairs={{0,15},{1,0},{2,1},{3,2},{4,3},{5,4},{6,5},{7,6},{8,7},{9,8},{10,9... | collective-permute-start | bytes 884744 | tf_op jit(solution)/shard_map/ppermute | solution.py:26
  143.5 8.7 %collective-permute-done.14 = bf16[32,4,9,128]{3,1,2,0:T(4,128)(2,1)S(1)} collective-permute-done((bf16[32,4,9,128]{3,1,2,0:T(4,128)(2,1)S(1)}, bf16[32,4,9,128]{3,1,2,0:T(4,128)(2,1)S(1)}, u32[]{:S(2)}, u32[]{:S(2)}) %collective-permute-start.14) | collective-permute-done | bytes 294944 | tf_op jit(solution)/shard_map/ppermute | solution.py:23
  155.1 3.2 broadcast_bitcast_fusion
  158.3 7.9 %reshape.164 = bf16[16,2,18432]{2,1,0:T(2,128)(2,1)} reshape(bf16[16,4,9,32,32]{4,3,2,1,0:T(8,128)(2,1)} %broadcast_bitcast_fusion) | data formatting | bytes 2359296
  166.2 4.4 all-to-all-start.1
  171.4 76.1 %while.15 = (s32[]{:T(128)}, f32[1,768]{1,0:T(1,128)S(1)}, f32[1,768]{1,0:T(1,128)S(1)}, f32[1,768,64]{1,2,0:T(8,128)S(1)}, s32[48]{0:T(128)S(1)}, /*index=5*/s3...) while((s32[]{:T(128)}, f32[1,768]{1,0:T(1,128)S(1)}, ...), condition=%wide.region_5.6_spmd.clone, body=%wide.region_0.5_spmd.clone.sunk | while | flops 106270224 | bytes 5566891 | solution.py:117
  172.6 4.7 conditional.3
  178.6 4.7 conditional.3
  184.6 4.7 conditional.3
  248.2 6.9 %reshape.165 = bf16[16,4,9,32,32]{4,3,2,1,0:T(8,128)(2,1)} reshape(bf16[16,2,18432]{2,1,0:T(2,128)(2,1)} %all-to-all-done.1) | data formatting | bytes 2359296
  255.0 3.1 bitcast_bitcast_fusion
  258.2 7.6 %copy.95 = bf16[32,4,9,16,32]{4,3,0,2,1:T(8,128)(2,1)} copy(bf16[32,4,9,16,32]{4,0,2,1,3:T(8,128)(2,1)S(1)} %bitcast_bitcast_fusion) | data formatting | bytes 2359296 | tf_op jit(solution)/shard_map/transpose | solution.py:34
  265.8 6.5 %reshape.124 = bf16[32,4,9,512]{3,0,2,1:T(8,128)(2,1)S(1)} reshape(bf16[32,4,9,16,32]{4,3,0,2,1:T(8,128)(2,1)} %copy.95) | data formatting | bytes 2359296 | tf_op jit(solution)/shard_map/reshape | solution.py:34
  273.7 215.4 %all-to-all-start.2 = ((bf16[32,4,9,128]{3,1,2,0:T(4,128)(2,1)}), bf16[32,4,9,128]{3,1,2,0:T(4,128)(2,1)S(1)}, u32[]{:S(2)}, u32[]{:S(2)}) async-start(bf16[32,4,9,128]{3,1,2,0:T(4,128)(2,1)} %copy.96), calls=%async_computation.2 | async-start | bytes 589824 | tf_op jit(solution)/shard_map/all_to_all | solution.py:159
  490.0 20.9 %all_gather.11 = bf16[192,512]{0,1:T(8,128)(2,1)S(1)} all-gather(bf16[192,32]{0,1:T(8,128)(2,1)S(1)} %fusion.25), channel_id=1, replica_groups=mesh['ep'=32,'tp'=16] {'tp'}, dimensions={1}, use_global_device_ids=true | all-gather | bytes 208896 | tf_op jit(solution)/shard_map/all_gather | solution.py:172
  (291 shorter events, 95.6 us)
Async XLA Ops:
  7.2 265.1 %copy-start = (bf16[4,512,128]{2,1,0:T(8,128)(2,1)S(1)}, bf16[4,512,128]{2,1,0:T(8,128)(2,1)}, u32[]{:S(2)}) copy-start(bf16[4,512,128]{2,1,0:T(8,128)(2,1)} %param.30) | copy-start | bytes 1572868
  7.2 164.1 %all-gather.4.cloned.1.call-start = ((), (), s32[]{:S(2)}) async-start(), calls=%async_computation.3 | async-start | bytes 6488064 | tf_op jit(solution)/shard_map/all_gather | solution.py:78
  62.6 12.8 %collective-permute-start = (bf16[32,4,9,128]{3,1,2,0:T(4,128)(2,1)S(1)}, bf16[32,4,9,128]{3,1,2,0:T(4,128)(2,1)S(1)}, u32[]{:S(2)}, u32[]{:S(2)}) collective-permute-start(bf16[32,4,9,128]{3,1,2,0:T(4,128)(2,1)S(1)} %all_to_all.15), channel_id=1, source_target_pairs={{0,1},{1,2},{2,3},{3,4},{4,5},{5,6},{6,7},{7,8},{8,9},{9,10},{10,1... | collective-permute-start | bytes 884744 | tf_op jit(solution)/shard_map/ppermute | solution.py:23
  65.7 11.7 %collective-permute-start.1 = (bf16[32,4,9,128]{3,1,2,0:T(4,128)(2,1)S(1)}, bf16[32,4,9,128]{3,1,2,0:T(4,128)(2,1)S(1)}, u32[]{:S(2)}, u32[]{:S(2)}) collective-permute-start(bf16[32,4,9,128]{3,1,2,0:T(4,128)(2,1)S(1)} %all_to_all.15), channel_id=1, source_target_pairs={{0,15},{1,0},{2,1},{3,2},{4,3},{5,4},{6,5},{7,6},{8,7},{9,8},{10,9... | collective-permute-start | bytes 884744 | tf_op jit(solution)/shard_map/ppermute | solution.py:26
  75.5 11.8 %collective-permute-start.2 = (bf16[32,4,9,128]{3,1,2,0:T(4,128)(2,1)S(1)}, bf16[32,4,9,128]{3,1,2,0:T(4,128)(2,1)S(1)}, u32[]{:S(2)}, u32[]{:S(2)}) collective-permute-start(bf16[32,4,9,128]{3,1,2,0:T(4,128)(2,1)S(1)} %collective-permute-done), channel_id=1, source_target_pairs={{0,1},{1,2},{2,3},{3,4},{4,5},{5,6},{6,7},{7,8},{8,9},{9,10},{10,1... | collective-permute-start | bytes 884744 | tf_op jit(solution)/shard_map/ppermute | solution.py:23
  77.4 11.8 %collective-permute-start.3 = (bf16[32,4,9,128]{3,1,2,0:T(4,128)(2,1)S(1)}, bf16[32,4,9,128]{3,1,2,0:T(4,128)(2,1)S(1)}, u32[]{:S(2)}, u32[]{:S(2)}) collective-permute-start(bf16[32,4,9,128]{3,1,2,0:T(4,128)(2,1)S(1)} %collective-permute-done.1), channel_id=1, source_target_pairs={{0,15},{1,0},{2,1},{3,2},{4,3},{5,4},{6,5},{7,6},{8,7},{9,8},{10,9... | collective-permute-start | bytes 884744 | tf_op jit(solution)/shard_map/ppermute | solution.py:26
  87.3 10.8 %collective-permute-start.4 = (bf16[32,4,9,128]{3,1,2,0:T(4,128)(2,1)S(1)}, bf16[32,4,9,128]{3,1,2,0:T(4,128)(2,1)S(1)}, u32[]{:S(2)}, u32[]{:S(2)}) collective-permute-start(bf16[32,4,9,128]{3,1,2,0:T(4,128)(2,1)S(1)} %collective-permute-done.2), channel_id=1, source_target_pairs={{0,1},{1,2},{2,3},{3,4},{4,5},{5,6},{6,7},{7,8},{8,9},{9,10},{10,1... | collective-permute-start | bytes 884744 | tf_op jit(solution)/shard_map/ppermute | solution.py:23
  89.2 10.8 %collective-permute-start.5 = (bf16[32,4,9,128]{3,1,2,0:T(4,128)(2,1)S(1)}, bf16[32,4,9,128]{3,1,2,0:T(4,128)(2,1)S(1)}, u32[]{:S(2)}, u32[]{:S(2)}) collective-permute-start(bf16[32,4,9,128]{3,1,2,0:T(4,128)(2,1)S(1)} %collective-permute-done.3), channel_id=1, source_target_pairs={{0,15},{1,0},{2,1},{3,2},{4,3},{5,4},{6,5},{7,6},{8,7},{9,8},{10,9... | collective-permute-start | bytes 884744 | tf_op jit(solution)/shard_map/ppermute | solution.py:26
  98.1 10.8 %collective-permute-start.6 = (bf16[32,4,9,128]{3,1,2,0:T(4,128)(2,1)S(1)}, bf16[32,4,9,128]{3,1,2,0:T(4,128)(2,1)S(1)}, u32[]{:S(2)}, u32[]{:S(2)}) collective-permute-start(bf16[32,4,9,128]{3,1,2,0:T(4,128)(2,1)S(1)} %collective-permute-done.4), channel_id=1, source_target_pairs={{0,1},{1,2},{2,3},{3,4},{4,5},{5,6},{6,7},{7,8},{8,9},{9,10},{10,1... | collective-permute-start | bytes 884744 | tf_op jit(solution)/shard_map/ppermute | solution.py:23
  100.0 10.8 %collective-permute-start.7 = (bf16[32,4,9,128]{3,1,2,0:T(4,128)(2,1)S(1)}, bf16[32,4,9,128]{3,1,2,0:T(4,128)(2,1)S(1)}, u32[]{:S(2)}, u32[]{:S(2)}) collective-permute-start(bf16[32,4,9,128]{3,1,2,0:T(4,128)(2,1)S(1)} %collective-permute-done.5), channel_id=1, source_target_pairs={{0,15},{1,0},{2,1},{3,2},{4,3},{5,4},{6,5},{7,6},{8,7},{9,8},{10,9... | collective-permute-start | bytes 884744 | tf_op jit(solution)/shard_map/ppermute | solution.py:26
  108.9 10.8 %collective-permute-start.8 = (bf16[32,4,9,128]{3,1,2,0:T(4,128)(2,1)S(1)}, bf16[32,4,9,128]{3,1,2,0:T(4,128)(2,1)S(1)}, u32[]{:S(2)}, u32[]{:S(2)}) collective-permute-start(bf16[32,4,9,128]{3,1,2,0:T(4,128)(2,1)S(1)} %collective-permute-done.6), channel_id=1, source_target_pairs={{0,1},{1,2},{2,3},{3,4},{4,5},{5,6},{6,7},{7,8},{8,9},{9,10},{10,1... | collective-permute-start | bytes 884744 | tf_op jit(solution)/shard_map/ppermute | solution.py:23
  110.8 10.8 %collective-permute-start.9 = (bf16[32,4,9,128]{3,1,2,0:T(4,128)(2,1)S(1)}, bf16[32,4,9,128]{3,1,2,0:T(4,128)(2,1)S(1)}, u32[]{:S(2)}, u32[]{:S(2)}) collective-permute-start(bf16[32,4,9,128]{3,1,2,0:T(4,128)(2,1)S(1)} %collective-permute-done.7), channel_id=1, source_target_pairs={{0,15},{1,0},{2,1},{3,2},{4,3},{5,4},{6,5},{7,6},{8,7},{9,8},{10,9... | collective-permute-start | bytes 884744 | tf_op jit(solution)/shard_map/ppermute | solution.py:26
  119.6 10.8 %collective-permute-start.10 = (bf16[32,4,9,128]{3,1,2,0:T(4,128)(2,1)S(1)}, bf16[32,4,9,128]{3,1,2,0:T(4,128)(2,1)S(1)}, u32[]{:S(2)}, u32[]{:S(2)}) collective-permute-start(bf16[32,4,9,128]{3,1,2,0:T(4,128)(2,1)S(1)} %collective-permute-done.8), channel_id=1, source_target_pairs={{0,1},{1,2},{2,3},{3,4},{4,5},{5,6},{6,7},{7,8},{8,9},{9,10},{10,1... | collective-permute-start | bytes 884744 | tf_op jit(solution)/shard_map/ppermute | solution.py:23
  121.6 10.8 %collective-permute-start.11 = (bf16[32,4,9,128]{3,1,2,0:T(4,128)(2,1)S(1)}, bf16[32,4,9,128]{3,1,2,0:T(4,128)(2,1)S(1)}, u32[]{:S(2)}, u32[]{:S(2)}) collective-permute-start(bf16[32,4,9,128]{3,1,2,0:T(4,128)(2,1)S(1)} %collective-permute-done.9), channel_id=1, source_target_pairs={{0,15},{1,0},{2,1},{3,2},{4,3},{5,4},{6,5},{7,6},{8,7},{9,8},{10,9... | collective-permute-start | bytes 884744 | tf_op jit(solution)/shard_map/ppermute | solution.py:26
  130.4 10.8 %collective-permute-start.12 = (bf16[32,4,9,128]{3,1,2,0:T(4,128)(2,1)S(1)}, bf16[32,4,9,128]{3,1,2,0:T(4,128)(2,1)S(1)}, u32[]{:S(2)}, u32[]{:S(2)}) collective-permute-start(bf16[32,4,9,128]{3,1,2,0:T(4,128)(2,1)S(1)} %collective-permute-done.10), channel_id=1, source_target_pairs={{0,1},{1,2},{2,3},{3,4},{4,5},{5,6},{6,7},{7,8},{8,9},{9,10},{10,1... | collective-permute-start | bytes 884744 | tf_op jit(solution)/shard_map/ppermute | solution.py:23
  132.3 11.1 %collective-permute-start.13 = (bf16[32,4,9,128]{3,1,2,0:T(4,128)(2,1)S(1)}, bf16[32,4,9,128]{3,1,2,0:T(4,128)(2,1)S(1)}, u32[]{:S(2)}, u32[]{:S(2)}) collective-permute-start(bf16[32,4,9,128]{3,1,2,0:T(4,128)(2,1)S(1)} %collective-permute-done.11), channel_id=1, source_target_pairs={{0,15},{1,0},{2,1},{3,2},{4,3},{5,4},{6,5},{7,6},{8,7},{9,8},{10,9... | collective-permute-start | bytes 884744 | tf_op jit(solution)/shard_map/ppermute | solution.py:26
  141.2 11.0 %collective-permute-start.14 = (bf16[32,4,9,128]{3,1,2,0:T(4,128)(2,1)S(1)}, bf16[32,4,9,128]{3,1,2,0:T(4,128)(2,1)S(1)}, u32[]{:S(2)}, u32[]{:S(2)}) collective-permute-start(bf16[32,4,9,128]{3,1,2,0:T(4,128)(2,1)S(1)} %collective-permute-done.12), channel_id=1, source_target_pairs={{0,1},{1,2},{2,3},{3,4},{4,5},{5,6},{6,7},{7,8},{8,9},{9,10},{10,1... | collective-permute-start | bytes 884744 | tf_op jit(solution)/shard_map/ppermute | solution.py:23
  166.2 82.0 %all-to-all-start.1 = ((bf16[16,2,18432]{2,1,0:T(2,128)(2,1)}), bf16[16,2,18432]{2,1,0:T(2,128)(2,1)}, u32[]{:S(2)}, u32[]{:S(2)}) async-start(bf16[16,2,18432]{2,1,0:T(2,128)(2,1)} %reshape.164), calls=%async_computation.1 | async-start | bytes 2359296 | tf_op jit(solution)/shard_map/all_to_all | solution.py:39
  170.6 345.7 %all-gather.6.cloned.1.call-start = ((), (), s32[]{:S(2)}) async-start(), calls=%async_computation.4 | async-start | bytes 1671168 | tf_op jit(solution)/shard_map/all_gather | solution.py:168
  265.8 223.5 %copy-start.4 = (bf16[2048,32]{0,1:T(8,128)(2,1)S(1)}, bf16[2048,32]{0,1:T(8,128)(2,1)}, u32[]{:S(2)}) copy-start(bf16[2048,32]{0,1:T(8,128)(2,1)} %param.31) | copy-start | bytes 393220
  265.8 223.8 %copy-start.5 = (bf16[2048,32]{0,1:T(8,128)(2,1)S(1)}, bf16[2048,32]{0,1:T(8,128)(2,1)}, u32[]{:S(2)}) copy-start(bf16[2048,32]{0,1:T(8,128)(2,1)} %param.32) | copy-start | bytes 393220
  272.3 243.1 %copy-start.3 = (bf16[512,128]{1,0:T(8,128)(2,1)S(1)}, bf16[512,128]{1,0:T(8,128)(2,1)}, u32[]{:S(2)}) copy-start(bf16[512,128]{1,0:T(8,128)(2,1)} %param.33) | copy-start | bytes 393220
  272.3 243.9 %copy-start.2 = (bf16[1024,128]{1,0:T(8,128)(2,1)S(1)}, bf16[1024,128]{1,0:T(8,128)(2,1)}, u32[]{:S(2)}) copy-start(bf16[1024,128]{1,0:T(8,128)(2,1)} %param.23) | copy-start | bytes 786436
  273.7 239.0 %all-to-all-start.2 = ((bf16[32,4,9,128]{3,1,2,0:T(4,128)(2,1)}), bf16[32,4,9,128]{3,1,2,0:T(4,128)(2,1)S(1)}, u32[]{:S(2)}, u32[]{:S(2)}) async-start(bf16[32,4,9,128]{3,1,2,0:T(4,128)(2,1)} %copy.96), calls=%async_computation.2 | async-start | bytes 589824 | tf_op jit(solution)/shard_map/all_to_all | solution.py:159
  (7 other events, 341.7 us)
Sparse Core Ops, SparseCore 0:
  10.7 92.1 all-gather.3
  248.3 262.0 all-gather.5
